TPU v7x, 256 devices: a 4x2x16 block of a 4x16x16 slice. The times are simulated.
256 devices in a mesh: grp: 2 (over y), fs: 16 (over z), tp: 8 (over x, core).
Axes of the slice: x: 4, y: 2, z: 16, core: 2. Of those that a mesh axis runs over, the one named last changes fastest.
The devices are a block of a 4x16x16 slice.
Arguments:
- tokens: bfloat16 [4096, 4096], P(('grp', 'tp')), parts along dimension 0, may hold values from -6 to 6
- routes: int32 [4096, 2], P(('grp', 'tp')), parts along dimension 0, may hold values from 0 to 7, all different within a row; in each aligned block of 256 rows (0 to 255, 256 to 511, ...) at most 128 rows name the same one
- route_weight: float32 [4096, 2], P(('grp', 'tp')), parts along dimension 0, may hold values from 0.2 to 1
- norm_gain: float32 [4096], P('fs'), may hold values from 0.1 to 1.9
- gate_train: float32 [8, 4096, 2048], P(None, 'fs', 'tp'), may hold values from -0.09375 to 0.09375
- up_train: float32 [8, 4096, 2048], P(None, 'fs', 'tp'), may hold values from -0.09375 to 0.09375
- down_train: float32 [8, 2048, 4096], P(None, 'fs', 'tp'), may hold values from -0.125 to 0.125
Outputs:
- gate_serve: bfloat16 [16, 4096, 2048], P(('grp', 'tp'), None, 'fs'), parts along dimension 0
- up_serve: bfloat16 [16, 4096, 2048], P(('grp', 'tp'), None, 'fs'), parts along dimension 0
- down_serve: bfloat16 [16, 2048, 4096], P(('grp', 'tp'), 'fs'), parts along dimension 0
- moe_out: bfloat16 [4096, 4096], P(('grp', 'tp'), 'fs'), parts along dimension 0
There are 2 independent parts, one for each index of `grp`. A program takes and returns all parts, laid end to end along the dimension named above; an argument that names none is the same for every part. Nothing has to cross between parts.
Inputs may be any that keep to these rules, and one draw needn't show every extreme that they name: `routes`: within the 256 rows of each device (aligned blocks), no expert is named by more than 128 rows, a bound that some block reaches; the two experts of a row differ; every expert is named somewhere.
All inputs are finite; a program needn't handle non-finite values.
Results may differ from a plain program's by a relative error of at most 0.0076.
Values may be sent and summed in bfloat16 or wider, within the bound.
No kernel may reach another device: no remote copies, remote signals or barrier semaphores. Data moves between devices by JAX's collectives and lax.ppermute only.
A program may use at most 128 MiB of HBM per device.

v0:
```python
import jax
import jax.numpy as jnp
from jax import lax
from jax.sharding import PartitionSpec as P

EXPERTS = 8
CAP = 128


def side_by_side(arrays, axis, split_dim, concat_dim, along):
    both = jnp.concatenate(arrays, axis=along)
    filled, at, gathered = (
        lax.all_to_all(both, axis, split_axis=split_dim, concat_axis=concat_dim, tiled=True),
        0,
        [],
    )
    for a in arrays:
        gathered.append(lax.slice_in_dim(filled, at, at + a.shape[along], axis=along))
        at += a.shape[along]
    return tuple(gathered)


def split_up(value, dim, length):
    lengths = value.shape
    tiles = value.reshape(*lengths[:dim], length, lengths[dim] // length, *lengths[dim + 1 :])
    return jnp.moveaxis(tiles, dim, 0)


def cut_rows(length, count):
    turn = length // count
    if turn >= 8:
        turn -= turn % 8
    return [turn * k for k in range(1, count)]


def laid_out(tiles, dim):
    lengths = list(tiles.shape[1:])
    lengths[dim] *= tiles.shape[0]
    return jnp.moveaxis(tiles, 0, dim).reshape(lengths)


def exchange_in_pieces(value, axis, pieces, split_dim, concat_dim):
    tiles = split_up(value, split_dim, lax.axis_size(axis))
    cut = max(range(1, max(2, tiles.ndim - 1)), key=lambda d: tiles.shape[d])
    gathered = []
    for slab in jnp.split(tiles, cut_rows(tiles.shape[cut], pieces), axis=cut):
        if slab.size:
            gathered.append(lax.all_to_all(slab, axis, split_axis=0, concat_axis=0, tiled=True))
    return laid_out(jnp.concatenate(gathered, axis=cut), concat_dim)


def per_device(tokens, routes, route_weight, norm_gain, gate_train, up_train, down_train):
    gate_cast = (norm_gain[None, :, None] * gate_train).astype(jnp.bfloat16)
    up_cast = (norm_gain[None, :, None] * up_train).astype(jnp.bfloat16)
    down_cast = down_train.astype(jnp.bfloat16)
    gate_mid, up_mid, down_serve = (
        *side_by_side((gate_cast, up_cast), "tp", 0, 2, 1),
        lax.all_to_all(down_cast, "tp", split_axis=0, concat_axis=2, tiled=True),
    )
    gate_serve, up_serve = side_by_side((gate_mid, up_mid), "fs", 2, 1, 0)
    tok_rows = tokens.shape[0]
    flat = routes.reshape(-1)
    expert_ids = jnp.arange(EXPERTS, dtype=jnp.int32)
    onehot = (flat[:, None] == expert_ids[None, :]).astype(jnp.int32)
    before = jnp.cumsum(onehot, axis=0) - onehot
    slot = jnp.sum(before * onehot, axis=1)
    place = (flat * CAP + slot).reshape(tok_rows, 2)
    slot_ids = jnp.arange(EXPERTS * CAP, dtype=jnp.int32)
    select = jnp.any(place[None, :, :] == slot_ids[:, None, None], axis=2).astype(jnp.bfloat16)
    outgoing = jnp.dot(select, tokens, preferred_element_type=jnp.float32).astype(jnp.bfloat16)
    arrived = lax.all_to_all(outgoing, "tp", split_axis=0, concat_axis=0, tiled=True)
    senders = lax.axis_size("tp")
    local = gate_serve.shape[0]
    arrived = arrived.reshape(senders, local, CAP, arrived.shape[1])
    gate_h = jnp.einsum("tlcd,ldf->tlcf", arrived, gate_serve, preferred_element_type=jnp.float32)
    up_h = jnp.einsum("tlcd,ldf->tlcf", arrived, up_serve, preferred_element_type=jnp.float32)
    hidden = (jax.nn.silu(gate_h) * up_h).astype(jnp.bfloat16)
    down_cols = exchange_in_pieces(down_serve, "fs", 2, 2, 1)
    empty = jnp.zeros((down_cols.shape[2], senders * local * CAP), jnp.float32)
    term = jnp.einsum(
        "tlcf,lfd->dtlc",
        lax.all_gather(hidden, "fs", axis=3, tiled=True),
        down_cols,
        preferred_element_type=jnp.float32,
    )
    summed = term.reshape(empty.shape)
    returned = lax.all_to_all(
        summed.astype(jnp.bfloat16), "tp", split_axis=1, concat_axis=1, tiled=True
    )
    picked = jnp.take(returned, place, axis=1)
    mixed = (
        picked[:, :, 0].astype(jnp.float32) * route_weight[None, :, 0]
        + picked[:, :, 1].astype(jnp.float32) * route_weight[None, :, 1]
    )
    moe_out = mixed.T.astype(jnp.bfloat16)
    return (gate_serve, up_serve, down_serve, moe_out)


def solution(mesh):
    return jax.shard_map(
        per_device,
        mesh=mesh,
        in_specs=(
            P(("grp", "tp"), None),
            P(("grp", "tp"), None),
            P(("grp", "tp"), None),
            P("fs"),
            P(None, "fs", "tp"),
            P(None, "fs", "tp"),
            P(None, "fs", "tp"),
        ),
        out_specs=(
            P(("grp", "tp"), None, "fs"),
            P(("grp", "tp"), None, "fs"),
            P(("grp", "tp"), "fs", None),
            P(("grp", "tp"), "fs"),
        ),
        check_vma=False,
    )
```

profile of v0, /device:TPU:33, one launch (start us, length us, event | category | flops | bytes accessed | tf_op | source)
XLA Modules:
  0.0 444.2 jit_solution(10201780460128886947)
XLA Ops:
  7.2 0.0 copy-start
  7.2 3.1 copy.96
  10.3 2.9 copy.97
  13.2 0.0 copy-done.5
  13.2 2.6 multiply_convert_fusion.1
  15.8 0.2 pad_maximum_fusion
  16.0 49.1 %all_to_all.82 = bf16[8,512,256]{1,2,0:T(8,128)(2,1)S(1)} all-to-all(bf16[8,512,256]{1,2,0:T(8,128)(2,1)S(1)} %pad_maximum_fusion), channel_id=1, replica_groups=mesh['grp'=2,'fs'=16,'tp'=8] {'tp'}, dimensions={0} | all-to-all | bytes 4194304 | tf_op jit(solution)/shard_map/all_to_all | solution.py:13
  65.1 0.1 fusion.12
  65.3 0.2 pad_maximum_fusion.1
  65.5 14.0 %copy.98 = bf16[2,256,2048]{1,0,2:T(2,128)(2,1)} copy(bf16[2,256,2048]{1,2,0:T(8,128)(2,1)S(1)} %pad_maximum_fusion.1) | data formatting | bytes 4194304 | tf_op jit(solution)/shard_map/concatenate | solution.py:11
  79.5 6.7 %all-to-all-start.1 = ((bf16[2,256,2048]{1,0,2:T(2,128)(2,1)}), bf16[2,256,2048]{1,0,2:T(2,128)(2,1)}, u32[]{:S(2)}, u32[]{:S(2)}) async-start(bf16[2,256,2048]{1,0,2:T(2,128)(2,1)} %copy.98), calls=%async_computation.1 | async-start | bytes 4194304 | tf_op jit(solution)/shard_map/all_to_all | solution.py:13
  86.2 0.0 copy-done.3
  86.2 0.1 copy.103
  86.3 0.1 eq.42
  86.5 0.1 eq.38
  86.6 1.1 reduce-window.6
  87.8 0.2 slice_reduce_fusion
  88.0 0.1 fusion.9
  88.1 0.1 reduce_sum.12
  88.3 0.1 copy.105
  88.4 0.4 fusion
  88.8 0.0 copy-done
  88.8 5.6 %convolution_convert_fusion = bf16[1024,4096]{1,0:T(8,128)(2,1)} fusion(pred[1024,256]{1,0:T(8,128)(4,1)S(1)} %fusion, bf16[256,4096]{1,0:T(8,128)(2,1)S(1)} %copy-done), kind=kOutput, calls=%fused_computation.1 | convolution fusion | flops 2151677952 | bytes 10747904 | tf_op jit(solution)/shard_map/dot_general | solution.py:70
  94.4 83.6 %all-to-all-done.1 = bf16[2,256,2048]{1,0,2:T(2,128)(2,1)} async-done(((bf16[2,256,2048]{1,0,2:T(2,128)(2,1)}), bf16[2,256,2048]{1,0,2:T(2,128)(2,1)}, u32[]{:S(2)}, u32[]{:S(2)}) %all-to-all-start.1) | async-done | bytes 2097184 | tf_op jit(solution)/shard_map/all_to_all | solution.py:13
  178.0 9.5 %all-to-all-start.5 = ((bf16[8,128,4096]{2,1,0:T(8,128)(2,1)}), bf16[8,128,4096]{2,1,0:T(8,128)(2,1)}, u32[]{:S(2)}, u32[]{:S(2)}) async-start(bf16[8,128,4096]{2,1,0:T(8,128)(2,1)} %bitcast.83), calls=%async_computation.5 | async-start | bytes 16777216 | tf_op jit(solution)/shard_map/all_to_all | solution.py:71
  187.5 0.0 all-gather.2.cloned.1.call-start
  187.5 1.9 copy.99
  189.4 0.1 fusion.11
  189.5 1.6 copy.110
  191.1 1.6 reshape.98
  192.6 1.6 copy.111
  194.2 2.3 reshape.99
  196.5 84.8 %all-to-all-done.5 = bf16[8,128,4096]{2,1,0:T(8,128)(2,1)} async-done(((bf16[8,128,4096]{2,1,0:T(8,128)(2,1)}), bf16[8,128,4096]{2,1,0:T(8,128)(2,1)}, u32[]{:S(2)}, u32[]{:S(2)}) %all-to-all-start.5) | async-done | bytes 8388640 | tf_op jit(solution)/shard_map/all_to_all | solution.py:71
  281.3 6.3 %convolution_bitcast_fusion.1 = f32[8,1,128,128]{2,3,0,1:T(8,128)S(1)} fusion(bf16[4096,128,1]{0,1,2:T(8,128)(2,1)S(1)} %reshape.98, bf16[8,128,4096]{2,1,0:T(8,128)(2,1)} %all-to-all-done.5), kind=kOutput, calls=%fused_computation.12 | convolution fusion | flops 1073741824 | bytes 9961472 | tf_op jit(solution)/shard_map/tlcd,ldf->tlcf/dot_general | solution.py:75
  287.7 0.0 copy-done.2
  287.7 7.1 %fusion.3 = bf16[8,1,128,128]{2,3,0,1:T(8,128)(2,1)} fusion(bf16[4096,128,1]{0,1,2:T(8,128)(2,1)S(1)} %copy-done.2, bf16[8,128,4096]{2,1,0:T(8,128)(2,1)} %all-to-all-done.5, f32[8,1,128,128]{2,3,0,1:T(8,128)S(1)} %convolution_bitcast_fusion.1), kind=kOutput, calls=%fused_computation.13 | convolution fusion | flops 1074528256 | bytes 10223616 | tf_op jit(solution)/shard_map/tlcd,ldf->tlcf/dot_general | solution.py:76
  294.7 0.1 all-gather.2.cloned.1.call-update
  294.8 2.5 copy.102
  297.4 19.4 %all_to_all.83 = bf16[8,128,512]{1,2,0:T(8,128)(2,1)S(1)} all-to-all(bf16[8,128,512]{1,2,0:T(8,128)(2,1)} %copy.102), channel_id=1, replica_groups=mesh['grp'=2,'fs'=16,'tp'=8] {'tp'}, dimensions={0} | all-to-all | bytes 2097152 | tf_op jit(solution)/shard_map/all_to_all | solution.py:58
  316.8 1.7 fusion.13
  318.5 2.4 copy.106
  320.9 7.1 %all-to-all-start.3 = ((bf16[16,1,64,256]{3,2,1,0:T(8,128)(2,1)}), bf16[16,1,64,256]{3,2,1,0:T(8,128)(2,1)}, u32[]{:S(2)}, u32[]{:S(2)}) async-start(bf16[16,1,64,256]{3,2,1,0:T(8,128)(2,1)} %copy.106), calls=%async_computation.3 | async-start | bytes 1048576 | tf_op jit(solution)/shard_map/all_to_all | solution.py:48
  328.0 2.4 copy.107
  330.4 27.1 %all-to-all-done.3 = bf16[16,1,64,256]{3,2,1,0:T(8,128)(2,1)} async-done(((bf16[16,1,64,256]{3,2,1,0:T(8,128)(2,1)}), bf16[16,1,64,256]{3,2,1,0:T(8,128)(2,1)}, u32[]{:S(2)}, u32[]{:S(2)}) %all-to-all-start.3) | async-done | bytes 524320 | tf_op jit(solution)/shard_map/all_to_all | solution.py:48
  357.5 40.3 %all_to_all.84 = bf16[16,1,64,256]{3,2,1,0:T(8,128)(2,1)S(1)} all-to-all(bf16[16,1,64,256]{3,2,1,0:T(8,128)(2,1)} %copy.107), channel_id=1, replica_groups=mesh['grp'=2,'fs'=16,'tp'=8] {'fs'}, dimensions={0} | all-to-all | bytes 1048576 | tf_op jit(solution)/shard_map/all_to_all | solution.py:48
  397.8 2.1 pad_maximum_fusion.2
  399.9 0.7 all-gather.2.cloned.1.call-done
  400.6 6.5 %copy.112 = bf16[8,1,128,2048]{3,2,0,1:T(8,128)(2,1)} copy(bf16[8,1,128,2048]{2,3,0,1:T(8,128)(2,1)} %all-gather.2.cloned.1.call-done) | data formatting | bytes 8388608 | tf_op jit(solution)/shard_map/all_gather | solution.py:82
  407.1 3.8 fusion.1
  410.9 0.0 copy-start.4
  410.9 0.9 copy.123
  411.8 11.8 %all-to-all-start.6 = ((bf16[256,8,128]{2,0,1:T(8,128)(2,1)}), bf16[256,8,128]{2,0,1:T(8,128)(2,1)}, u32[]{:S(2)}, u32[]{:S(2)}) async-start(bf16[256,8,128]{2,0,1:T(8,128)(2,1)} %bitcast.89), calls=%async_computation.6 | async-start | bytes 1048576 | tf_op jit(solution)/shard_map/all_to_all | solution.py:87
  423.7 0.1 copy.115
  423.8 0.1 reshape.90
  424.0 1.3 copy.117
  425.3 1.3 copy.100
  426.6 1.3 copy.101
  427.9 5.2 %all-to-all-done.6 = bf16[256,8,128]{2,0,1:T(8,128)(2,1)} async-done(((bf16[256,8,128]{2,0,1:T(8,128)(2,1)}), bf16[256,8,128]{2,0,1:T(8,128)(2,1)}, u32[]{:S(2)}, u32[]{:S(2)}) %all-to-all-start.6) | async-done | bytes 524320 | tf_op jit(solution)/shard_map/all_to_all | solution.py:87
  433.1 1.2 copy.114
  434.4 0.0 copy-start.1
  434.4 2.0 gather_fusion
  436.3 0.1 reshape.93
  436.4 0.1 fusion.6
  436.6 0.8 fusion.7
  (12 shorter events, 0.1 us)
Async XLA Ops:
  7.2 81.6 %copy-start = (bf16[256,4096]{1,0:T(8,128)(2,1)S(1)}, bf16[256,4096]{1,0:T(8,128)(2,1)}, u32[]{:S(2)}) copy-start(bf16[256,4096]{1,0:T(8,128)(2,1)} %param.7) | copy-start | bytes 6291460
  10.3 2.9 copy-start.5
  79.5 6.7 %copy-start.3 = (s32[256,2]{0,1:T(2,128)S(1)}, s32[256,2]{0,1:T(2,128)}, u32[]{:S(2)}) copy-start(s32[256,2]{0,1:T(2,128)} %param.8) | copy-start | bytes 6148
  79.5 98.5 %all-to-all-start.1 = ((bf16[2,256,2048]{1,0,2:T(2,128)(2,1)}), bf16[2,256,2048]{1,0,2:T(2,128)(2,1)}, u32[]{:S(2)}, u32[]{:S(2)}) async-start(bf16[2,256,2048]{1,0,2:T(2,128)(2,1)} %copy.98), calls=%async_computation.1 | async-start | bytes 4194304 | tf_op jit(solution)/shard_map/all_to_all | solution.py:13
  178.0 103.3 %all-to-all-start.5 = ((bf16[8,128,4096]{2,1,0:T(8,128)(2,1)}), bf16[8,128,4096]{2,1,0:T(8,128)(2,1)}, u32[]{:S(2)}, u32[]{:S(2)}) async-start(bf16[8,128,4096]{2,1,0:T(8,128)(2,1)} %bitcast.83), calls=%async_computation.5 | async-start | bytes 16777216 | tf_op jit(solution)/shard_map/all_to_all | solution.py:71
  187.5 213.1 %all-gather.2.cloned.1.call-start = ((), (), s32[]{:S(2)}) async-start(), calls=%async_computation.7 | async-start | bytes 4456448 | tf_op jit(solution)/shard_map/all_gather | solution.py:82
  281.3 6.4 %copy-start.2 = (bf16[4096,128,1]{0,1,2:T(8,128)(2,1)S(1)}, bf16[4096,128,1]{0,1,2:T(8,128)(2,1)}, u32[]{:S(2)}) copy-start(bf16[4096,128,1]{0,1,2:T(8,128)(2,1)} %reshape.99) | copy-start | bytes 3145732
  320.9 36.6 %all-to-all-start.3 = ((bf16[16,1,64,256]{3,2,1,0:T(8,128)(2,1)}), bf16[16,1,64,256]{3,2,1,0:T(8,128)(2,1)}, u32[]{:S(2)}, u32[]{:S(2)}) async-start(bf16[16,1,64,256]{3,2,1,0:T(8,128)(2,1)} %copy.106), calls=%async_computation.3 | async-start | bytes 1048576 | tf_op jit(solution)/shard_map/all_to_all | solution.py:48
  410.9 13.1 %copy-start.4 = (f32[256,2]{0,1:T(2,128)S(1)}, f32[256,2]{0,1:T(2,128)}, u32[]{:S(2)}) copy-start(f32[256,2]{0,1:T(2,128)} %param.9) | copy-start | bytes 6148
  411.8 21.3 %all-to-all-start.6 = ((bf16[256,8,128]{2,0,1:T(8,128)(2,1)}), bf16[256,8,128]{2,0,1:T(8,128)(2,1)}, u32[]{:S(2)}, u32[]{:S(2)}) async-start(bf16[256,8,128]{2,0,1:T(8,128)(2,1)} %bitcast.89), calls=%async_computation.6 | async-start | bytes 1048576 | tf_op jit(solution)/shard_map/all_to_all | solution.py:87
  434.4 3.0 copy-start.1
Sparse Core Ops, SparseCore 0:
  294.9 105.5 all-gather.1
where the time goes:
time: 445 us; the launch traced here: 444 us
  waiting for transfers between devices  202 us (45%)
  blocking collectives  109 us (24%)
  local copies, waits for them, and re-layouts  53.9 us (12%)
  starting transfers between devices  35.2 us (8%)
  matrix products  22.8 us (5%)
  between operations  14.3 us (3%)
  other arithmetic  7.73 us (2%)
    all_to_all x1, waiting for transfers between devices, per_device(): lax.all_to_all(outgoing, 'tp', split_axis=0, concat_axis=0, tiled=True)  84.8 us
    all_to_all x1, waiting for transfers between devices, side_by_side(): lax.all_to_all(both, axis, split_axis=split_dim, concat_axis=concat_dim,...  83.6 us
    all_to_all x1, blocking collectives, side_by_side(): lax.all_to_all(both, axis, split_axis=split_dim, concat_axis=concat_dim,...  49.1 us
    all_to_all x1, blocking collectives, exchange_in_pieces(): lax.all_to_all(slab, axis, split_axis=0, concat_axis=0, tiled=True)  40.3 us
    all_to_all x1, waiting for transfers between devices, exchange_in_pieces(): lax.all_to_all(slab, axis, split_axis=0, concat_axis=0, tiled=True)  27.1 us
    all_to_all x1, blocking collectives, per_device(): lax.all_to_all(down_cast, 'tp', split_axis=0, concat_axis=2, tiled=True)  19.4 us
    concatenate x1, local copies, waits for them, and re-layouts, side_by_side(): both = jnp.concatenate(arrays, axis=along)  14 us
    all_to_all x1, starting transfers between devices, per_device(): lax.all_to_all(summed.astype(jnp.bfloat16), 'tp', split_axis=1, concat_ax...  11.8 us
  transfers between devices with their start and end apart: 5, of which 5 were waited for; matrix products, arithmetic and copies ran while one was open for 7% of the time, Pallas kernels for 0%

commit v1 on v0

--- a/solution.py
+++ b/solution.py
@@ -1,10 +1,21 @@
+import functools
 import jax
 import jax.numpy as jnp
 from jax import lax
 from jax.sharding import PartitionSpec as P
+from jax.lax import all_to_all, axis_size
 
 EXPERTS = 8
 CAP = 128
+
+
+def enter_indices(m, axis_id):
+    return jnp.concatenate(
+        all_to_all(jnp.stack(jnp.split(m, axis_size(axis_id), axis=1)), axis_id, 0, 0), axis=1
+    )
+
+
+review_tails_here = functools.partial(enter_indices, axis_id="tp")
 
 
 def side_by_side(arrays, axis, split_dim, concat_dim, along):
@@ -84,9 +95,7 @@
         preferred_element_type=jnp.float32,
     )
     summed = term.reshape(empty.shape)
-    returned = lax.all_to_all(
-        summed.astype(jnp.bfloat16), "tp", split_axis=1, concat_axis=1, tiled=True
-    )
+    returned = review_tails_here(summed.astype(jnp.bfloat16))
     picked = jnp.take(returned, place, axis=1)
     mixed = (
         picked[:, :, 0].astype(jnp.float32) * route_weight[None, :, 0]

time: 445 us -> 450 us (1.011)
    unnamed x17 -> x24, local copies, waits for them, and re-layouts: 10 us -> 14.5 us
where the time goes in v1:
time: 450 us; the launch traced here: 449 us
  waiting for transfers between devices  202 us (45%)
  blocking collectives  109 us (24%)
  local copies, waits for them, and re-layouts  58.2 us (13%)
  starting transfers between devices  35.2 us (8%)
  matrix products  22.8 us (5%)
  between operations  14.3 us (3%)
  other arithmetic  7.73 us (2%)
    all_to_all x1, waiting for transfers between devices, per_device(): lax.all_to_all(outgoing, 'tp', split_axis=0, concat_axis=0, tiled=True)  84.8 us
    all_to_all x1, waiting for transfers between devices, side_by_side(): lax.all_to_all(both, axis, split_axis=split_dim, concat_axis=concat_dim,...  83.6 us
    all_to_all x1, blocking collectives, side_by_side(): lax.all_to_all(both, axis, split_axis=split_dim, concat_axis=concat_dim,...  49.1 us
    all_to_all x1, blocking collectives, exchange_in_pieces(): lax.all_to_all(slab, axis, split_axis=0, concat_axis=0, tiled=True)  40.3 us
    all_to_all x1, waiting for transfers between devices, exchange_in_pieces(): lax.all_to_all(slab, axis, split_axis=0, concat_axis=0, tiled=True)  27.1 us
    all_to_all x1, blocking collectives, per_device(): lax.all_to_all(down_cast, 'tp', split_axis=0, concat_axis=2, tiled=True)  19.4 us
    unnamed x24, local copies, waits for them, and re-layouts  14.5 us
    concatenate x1, local copies, waits for them, and re-layouts, side_by_side(): both = jnp.concatenate(arrays, axis=along)  14 us
  transfers between devices with their start and end apart: 5, of which 5 were waited for; matrix products, arithmetic and copies ran while one was open for 7% of the time, Pallas kernels for 0%

profile of v1, /device:TPU:33, one launch (start us, length us, event | category | flops | bytes accessed | tf_op | source)
XLA Modules:
  0.0 448.5 jit_solution(4103921136115488898)
XLA Ops:
  7.2 0.0 copy-start
  7.2 3.1 copy.93
  10.3 2.9 copy.94
  13.2 2.6 multiply_convert_fusion.1
  15.8 0.2 pad_maximum_fusion
  16.0 49.1 %all_to_all.75 = bf16[8,512,256]{1,2,0:T(8,128)(2,1)S(1)} all-to-all(bf16[8,512,256]{1,2,0:T(8,128)(2,1)S(1)} %pad_maximum_fusion), channel_id=1, replica_groups=mesh['grp'=2,'fs'=16,'tp'=8] {'tp'}, dimensions={0} | all-to-all | bytes 4194304 | tf_op jit(solution)/shard_map/all_to_all | solution.py:24
  65.1 0.1 fusion.19
  65.3 0.2 pad_maximum_fusion.1
  65.5 14.0 %copy.95 = bf16[2,256,2048]{1,0,2:T(2,128)(2,1)} copy(bf16[2,256,2048]{1,2,0:T(8,128)(2,1)S(1)} %pad_maximum_fusion.1) | data formatting | bytes 4194304 | tf_op jit(solution)/shard_map/concatenate | solution.py:22
  79.5 6.7 %all-to-all-start.1 = ((bf16[2,256,2048]{1,0,2:T(2,128)(2,1)}), bf16[2,256,2048]{1,0,2:T(2,128)(2,1)}, u32[]{:S(2)}, u32[]{:S(2)}) async-start(bf16[2,256,2048]{1,0,2:T(2,128)(2,1)} %copy.95), calls=%async_computation.1 | async-start | bytes 4194304 | tf_op jit(solution)/shard_map/all_to_all | solution.py:24
  86.2 0.1 copy.100
  86.3 0.1 eq.42
  86.5 0.1 eq.38
  86.6 1.1 reduce-window.6
  87.8 0.2 slice_reduce_fusion
  88.0 0.1 fusion.16
  88.1 0.1 reduce_sum.12
  88.3 0.1 copy.102
  88.4 0.4 fusion
  88.8 5.6 %convolution_convert_fusion = bf16[1024,4096]{1,0:T(8,128)(2,1)} fusion(pred[1024,256]{1,0:T(8,128)(4,1)S(1)} %fusion, bf16[256,4096]{1,0:T(8,128)(2,1)S(1)} %copy-done), kind=kOutput, calls=%fused_computation.1 | convolution fusion | flops 2151677952 | bytes 10747904 | tf_op jit(solution)/shard_map/dot_general | solution.py:81
  94.4 83.6 %all-to-all-done.1 = bf16[2,256,2048]{1,0,2:T(2,128)(2,1)} async-done(((bf16[2,256,2048]{1,0,2:T(2,128)(2,1)}), bf16[2,256,2048]{1,0,2:T(2,128)(2,1)}, u32[]{:S(2)}, u32[]{:S(2)}) %all-to-all-start.1) | async-done | bytes 2097184 | tf_op jit(solution)/shard_map/all_to_all | solution.py:24
  178.0 9.5 %all-to-all-start.5 = ((bf16[8,128,4096]{2,1,0:T(8,128)(2,1)}), bf16[8,128,4096]{2,1,0:T(8,128)(2,1)}, u32[]{:S(2)}, u32[]{:S(2)}) async-start(bf16[8,128,4096]{2,1,0:T(8,128)(2,1)} %bitcast.111), calls=%async_computation.5 | async-start | bytes 16777216 | tf_op jit(solution)/shard_map/all_to_all | solution.py:82
  187.5 1.9 copy.96
  189.4 0.1 fusion.18
  189.5 1.6 copy.107
  191.1 1.6 reshape.104
  192.6 1.6 copy.108
  194.2 2.3 reshape.105
  196.5 84.8 %all-to-all-done.5 = bf16[8,128,4096]{2,1,0:T(8,128)(2,1)} async-done(((bf16[8,128,4096]{2,1,0:T(8,128)(2,1)}), bf16[8,128,4096]{2,1,0:T(8,128)(2,1)}, u32[]{:S(2)}, u32[]{:S(2)}) %all-to-all-start.5) | async-done | bytes 8388640 | tf_op jit(solution)/shard_map/all_to_all | solution.py:82
  281.3 6.3 %convolution_bitcast_fusion.1 = f32[8,1,128,128]{2,3,0,1:T(8,128)S(1)} fusion(bf16[4096,128,1]{0,1,2:T(8,128)(2,1)S(1)} %reshape.104, bf16[8,128,4096]{2,1,0:T(8,128)(2,1)} %all-to-all-done.5), kind=kOutput, calls=%fused_computation.11 | convolution fusion | flops 1073741824 | bytes 9961472 | tf_op jit(solution)/shard_map/tlcd,ldf->tlcf/dot_general | solution.py:86
  287.7 7.1 %fusion.2 = bf16[8,1,128,128]{2,3,0,1:T(8,128)(2,1)} fusion(bf16[4096,128,1]{0,1,2:T(8,128)(2,1)S(1)} %copy-done.2, bf16[8,128,4096]{2,1,0:T(8,128)(2,1)} %all-to-all-done.5, f32[8,1,128,128]{2,3,0,1:T(8,128)S(1)} %convolution_bitcast_fusion.1), kind=kOutput, calls=%fused_computation.12 | convolution fusion | flops 1074528256 | bytes 10223616 | tf_op jit(solution)/shard_map/tlcd,ldf->tlcf/dot_general | solution.py:87
  294.7 0.1 all-gather.2.cloned.1.call-update
  294.8 2.5 copy.99
  297.4 19.4 %all_to_all.76 = bf16[8,128,512]{1,2,0:T(8,128)(2,1)S(1)} all-to-all(bf16[8,128,512]{1,2,0:T(8,128)(2,1)} %copy.99), channel_id=1, replica_groups=mesh['grp'=2,'fs'=16,'tp'=8] {'tp'}, dimensions={0} | all-to-all | bytes 2097152 | tf_op jit(solution)/shard_map/all_to_all | solution.py:69
  316.8 1.7 fusion.20
  318.5 2.4 copy.103
  320.9 7.1 %all-to-all-start.3 = ((bf16[16,1,64,256]{3,2,1,0:T(8,128)(2,1)}), bf16[16,1,64,256]{3,2,1,0:T(8,128)(2,1)}, u32[]{:S(2)}, u32[]{:S(2)}) async-start(bf16[16,1,64,256]{3,2,1,0:T(8,128)(2,1)} %copy.103), calls=%async_computation.3 | async-start | bytes 1048576 | tf_op jit(solution)/shard_map/all_to_all | solution.py:59
  328.0 2.4 copy.104
  330.4 27.1 %all-to-all-done.3 = bf16[16,1,64,256]{3,2,1,0:T(8,128)(2,1)} async-done(((bf16[16,1,64,256]{3,2,1,0:T(8,128)(2,1)}), bf16[16,1,64,256]{3,2,1,0:T(8,128)(2,1)}, u32[]{:S(2)}, u32[]{:S(2)}) %all-to-all-start.3) | async-done | bytes 524320 | tf_op jit(solution)/shard_map/all_to_all | solution.py:59
  357.5 40.3 %all_to_all.77 = bf16[16,1,64,256]{3,2,1,0:T(8,128)(2,1)S(1)} all-to-all(bf16[16,1,64,256]{3,2,1,0:T(8,128)(2,1)} %copy.104), channel_id=1, replica_groups=mesh['grp'=2,'fs'=16,'tp'=8] {'fs'}, dimensions={0} | all-to-all | bytes 1048576 | tf_op jit(solution)/shard_map/all_to_all | solution.py:59
  397.8 2.1 pad_maximum_fusion.2
  399.9 0.7 all-gather.2.cloned.1.call-done
  400.6 6.5 %copy.109 = bf16[8,1,128,2048]{3,2,0,1:T(8,128)(2,1)} copy(bf16[8,1,128,2048]{2,3,0,1:T(8,128)(2,1)} %all-gather.2.cloned.1.call-done) | data formatting | bytes 8388608 | tf_op jit(solution)/shard_map/all_gather | solution.py:93
  407.1 3.8 convolution_convert_fusion.1
  410.9 0.6 fusion.14
  411.6 0.6 fusion.13
  412.2 0.6 fusion.12
  412.8 0.6 fusion.11
  413.5 0.6 fusion.10
  414.1 0.7 fusion.9
  414.8 0.6 fusion.8
  415.4 0.6 fusion.7
  416.1 11.8 %all-to-all-start.6 = ((bf16[8,256,128]{2,1,0:T(8,128)(2,1)}), bf16[8,256,128]{2,1,0:T(8,128)(2,1)}, u32[]{:S(2)}, u32[]{:S(2)}) async-start(bf16[8,256,128]{2,1,0:T(8,128)(2,1)} %fusion.7), calls=%async_computation.6 | async-start | bytes 1048576 | tf_op jit(solution)/shard_map/all_to_all | solution.py:14
  427.9 0.1 copy.111
  428.1 0.1 reshape.96
  428.3 1.3 copy.113
  429.6 1.3 copy.97
  430.9 1.3 copy.98
  432.2 5.2 %all-to-all-done.6 = bf16[8,256,128]{2,1,0:T(8,128)(2,1)} async-done(((bf16[8,256,128]{2,1,0:T(8,128)(2,1)}), bf16[8,256,128]{2,1,0:T(8,128)(2,1)}, u32[]{:S(2)}, u32[]{:S(2)}) %all-to-all-start.6) | async-done | bytes 524320 | tf_op jit(solution)/shard_map/all_to_all | solution.py:14
  437.4 1.2 copy.110
  438.6 2.0 gather_fusion
  440.6 0.1 reshape.99
  440.7 0.1 fusion.5
  440.9 0.8 fusion.6
  (19 shorter events, 0.1 us)
Async XLA Ops:
  7.2 81.6 %copy-start = (bf16[256,4096]{1,0:T(8,128)(2,1)S(1)}, bf16[256,4096]{1,0:T(8,128)(2,1)}, u32[]{:S(2)}) copy-start(bf16[256,4096]{1,0:T(8,128)(2,1)} %param.7) | copy-start | bytes 6291460
  10.3 2.9 copy-start.5
  79.5 6.7 %copy-start.3 = (s32[256,2]{0,1:T(2,128)S(1)}, s32[256,2]{0,1:T(2,128)}, u32[]{:S(2)}) copy-start(s32[256,2]{0,1:T(2,128)} %param.8) | copy-start | bytes 6148
  79.5 98.5 %all-to-all-start.1 = ((bf16[2,256,2048]{1,0,2:T(2,128)(2,1)}), bf16[2,256,2048]{1,0,2:T(2,128)(2,1)}, u32[]{:S(2)}, u32[]{:S(2)}) async-start(bf16[2,256,2048]{1,0,2:T(2,128)(2,1)} %copy.95), calls=%async_computation.1 | async-start | bytes 4194304 | tf_op jit(solution)/shard_map/all_to_all | solution.py:24
  178.0 103.3 %all-to-all-start.5 = ((bf16[8,128,4096]{2,1,0:T(8,128)(2,1)}), bf16[8,128,4096]{2,1,0:T(8,128)(2,1)}, u32[]{:S(2)}, u32[]{:S(2)}) async-start(bf16[8,128,4096]{2,1,0:T(8,128)(2,1)} %bitcast.111), calls=%async_computation.5 | async-start | bytes 16777216 | tf_op jit(solution)/shard_map/all_to_all | solution.py:82
  187.5 213.1 %all-gather.2.cloned.1.call-start = ((), (), s32[]{:S(2)}) async-start(), calls=%async_computation.7 | async-start | bytes 4456448 | tf_op jit(solution)/shard_map/all_gather | solution.py:93
  281.3 6.4 %copy-start.2 = (bf16[4096,128,1]{0,1,2:T(8,128)(2,1)S(1)}, bf16[4096,128,1]{0,1,2:T(8,128)(2,1)}, u32[]{:S(2)}) copy-start(bf16[4096,128,1]{0,1,2:T(8,128)(2,1)} %reshape.105) | copy-start | bytes 3145732
  320.9 36.6 %all-to-all-start.3 = ((bf16[16,1,64,256]{3,2,1,0:T(8,128)(2,1)}), bf16[16,1,64,256]{3,2,1,0:T(8,128)(2,1)}, u32[]{:S(2)}, u32[]{:S(2)}) async-start(bf16[16,1,64,256]{3,2,1,0:T(8,128)(2,1)} %copy.103), calls=%async_computation.3 | async-start | bytes 1048576 | tf_op jit(solution)/shard_map/all_to_all | solution.py:59
  410.9 17.3 %copy-start.4 = (f32[256,2]{0,1:T(2,128)S(1)}, f32[256,2]{0,1:T(2,128)}, u32[]{:S(2)}) copy-start(f32[256,2]{0,1:T(2,128)} %param.9) | copy-start | bytes 6148
  416.1 21.3 %all-to-all-start.6 = ((bf16[8,256,128]{2,1,0:T(8,128)(2,1)}), bf16[8,256,128]{2,1,0:T(8,128)(2,1)}, u32[]{:S(2)}, u32[]{:S(2)}) async-start(bf16[8,256,128]{2,1,0:T(8,128)(2,1)} %fusion.7), calls=%async_computation.6 | async-start | bytes 1048576 | tf_op jit(solution)/shard_map/all_to_all | solution.py:14
  438.6 3.0 copy-start.1
Sparse Core Ops, SparseCore 0:
  294.9 105.5 all-gather.1
